TPU v7x, 32 devices: a whole 2x2x4 slice. The times are simulated.
32 devices in a mesh: fs: 16 (over z, y, x), tp: 2 (over core).
Axes of the slice: x: 2, y: 2, z: 4, core: 2. Of those that a mesh axis runs over, the one named last changes fastest.
Arguments:
- tokens: bfloat16 [2, 256, 2048], P('tp'), may hold values from -6 to 6
- gain_first: float32 [2048], P('fs'), may hold values from 0.1 to 1.9
- gate_first: float32 [2048, 5632], P('fs', 'tp'), may hold values from -0.125 to 0.125
- up_first: float32 [2048, 5632], P('fs', 'tp'), may hold values from -0.125 to 0.125
- down_first: float32 [2048, 5632], P('fs', 'tp'), may hold values from -0.3125 to 0.3125
- gain_second: float32 [2048], P('fs'), may hold values from 0.1 to 1.9
- gate_second: float32 [2048, 5632], P('fs', 'tp'), may hold values from -0.125 to 0.125
- up_second: float32 [2048, 5632], P('fs', 'tp'), may hold values from -0.125 to 0.125
- down_second: float32 [2048, 5632], P('fs', 'tp'), may hold values from -0.3125 to 0.3125
Outputs:
- mixed: bfloat16 [2, 256, 2048], P('tp', 'fs')
- served_gate_first: bfloat16 [2, 2816, 2048], P(None, 'fs')
- served_up_first: bfloat16 [2, 2816, 2048], P(None, 'fs')
- served_down_first: bfloat16 [2, 2816, 2048], P(None, 'fs')
- served_gate_second: bfloat16 [2, 2816, 2048], P(None, 'fs')
- served_up_second: bfloat16 [2, 2816, 2048], P(None, 'fs')
- served_down_second: bfloat16 [2, 2816, 2048], P(None, 'fs')
All inputs are finite; a program needn't handle non-finite values.
Results may differ from a plain program's by a relative error of at most 0.013.
Values may be sent and summed in bfloat16 or wider, within the bound.
A program may use at most 64 MiB of HBM per device.

v0:
```python
import jax
import jax.numpy as jnp
from jax import lax
from jax.sharding import PartitionSpec as P


def normalize(values):
    wide = values.astype(jnp.float32)
    scale = lax.rsqrt(jnp.mean(wide * wide, axis=-1, keepdims=True) + 1e-06)
    return (wide * scale).astype(jnp.bfloat16)


def folded(weight, gain):
    return (weight * gain[:, None]).astype(jnp.bfloat16).T


def relayout(gate_part, up_part, down_part):
    gate_cut, up_cut, down_cut = (
        lax.all_to_all(gate_part, "fs", split_axis=0, concat_axis=1, tiled=True),
        lax.all_to_all(up_part, "fs", split_axis=0, concat_axis=1, tiled=True),
        lax.all_to_all(down_part, "fs", split_axis=0, concat_axis=1, tiled=True),
    )
    return (
        lax.all_gather(gate_cut[None], "tp", axis=0, tiled=True),
        lax.all_gather(up_cut[None], "tp", axis=0, tiled=True),
        lax.all_gather(down_cut[None], "tp", axis=0, tiled=True),
    )


def hidden_of(normed, gate_served, up_served):
    gate_flat = gate_served.reshape(-1, gate_served.shape[2])
    up_flat = up_served.reshape(-1, up_served.shape[2])
    gate_act = jnp.einsum("rd,hd->rh", normed, gate_flat, preferred_element_type=jnp.float32)
    up_act = jnp.einsum("rd,hd->rh", normed, up_flat, preferred_element_type=jnp.float32)
    return (jax.nn.silu(gate_act) * up_act).astype(jnp.bfloat16)


def projector(hidden, down_flat):
    return jnp.dot(hidden, down_flat, preferred_element_type=jnp.float32)


def shards(
    tokens,
    gain_first,
    gate_first,
    up_first,
    down_first,
    gain_second,
    gate_second,
    up_second,
    down_second,
):
    gate_one, up_one, down_one = relayout(
        folded(gate_first, gain_first),
        folded(up_first, gain_first),
        down_first.astype(jnp.bfloat16).T,
    )
    gate_two, up_two, down_two = relayout(
        folded(gate_second, gain_second),
        folded(up_second, gain_second),
        down_second.astype(jnp.bfloat16).T,
    )
    rows = tokens[0]
    keep = rows.shape[0] // lax.axis_size("fs")
    offset = lax.axis_index("fs") * keep
    hidden_first = hidden_of(normalize(rows), gate_one, up_one)
    down_flat_one = down_one.reshape(-1, down_one.shape[2])
    partial_value = jnp.dot(hidden_first, down_flat_one, preferred_element_type=jnp.float32)
    branch = lax.psum(partial_value, "fs")
    whole_middle = (rows.astype(jnp.float32) + 0.5 * branch).astype(jnp.bfloat16)
    hidden_second = hidden_of(normalize(whole_middle), gate_two, up_two)
    middle = lax.dynamic_slice_in_dim(whole_middle, offset, keep, 0)
    down_flat_two = down_two.reshape(-1, down_two.shape[2])
    branch_two = lax.psum_scatter(
        projector(hidden_second, down_flat_two), "fs", scatter_dimension=0, tiled=True
    )
    mixed = (middle.astype(jnp.float32) + 0.5 * branch_two).astype(jnp.bfloat16)[None]
    return (mixed, gate_one, up_one, down_one, gate_two, up_two, down_two)


def solution(mesh):
    return jax.shard_map(
        shards,
        mesh=mesh,
        in_specs=(
            P("tp", None, None),
            P("fs"),
            P("fs", "tp"),
            P("fs", "tp"),
            P("fs", "tp"),
            P("fs"),
            P("fs", "tp"),
            P("fs", "tp"),
            P("fs", "tp"),
        ),
        out_specs=(
            P("tp", "fs", None),
            P(None, "fs", None),
            P(None, "fs", None),
            P(None, "fs", None),
            P(None, "fs", None),
            P(None, "fs", None),
            P(None, "fs", None),
        ),
        check_vma=False,
    )
```

profile of v0, /device:TPU:0, one launch (start us, length us, event | category | flops | bytes accessed | tf_op | source)
XLA Modules:
  0.0 395.1 jit_solution(5311903597791260053)
XLA Ops:
  7.2 1.8 copy.40
  9.0 1.8 copy.42
  10.8 1.1 multiply_convert_fusion.3
  11.9 28.1 %all_to_all.96 = bf16[16,176,128]{2,1,0:T(8,128)(2,1)S(1)} all-to-all(bf16[16,176,128]{2,1,0:T(8,128)(2,1)S(1)} %bitcast.56), channel_id=1, replica_groups=mesh['fs'=16,'tp'=2] {'fs'}, dimensions={0} | all-to-all | bytes 1441792 | tf_op jit(solution)/shard_map/all_to_all | solution.py:19
  40.3 1.2 broadcast_in_dim.27
  41.5 22.3 %all_to_all.97 = bf16[16,176,128]{2,1,0:T(8,128)(2,1)S(1)} all-to-all(bf16[16,176,128]{2,1,0:T(8,128)(2,1)S(1)} %bitcast.54), channel_id=1, replica_groups=mesh['fs'=16,'tp'=2] {'fs'}, dimensions={0} | all-to-all | bytes 1441792 | tf_op jit(solution)/shard_map/all_to_all | solution.py:20
  64.0 1.2 broadcast_in_dim.28
  65.3 0.4 copy-done.3
  65.7 0.4 copy.44
  66.0 22.3 %all_to_all.98 = bf16[16,176,128]{2,1,0:T(8,128)(2,1)S(1)} all-to-all(bf16[16,176,128]{2,1,0:T(8,128)(2,1)S(1)} %bitcast.64), channel_id=1, replica_groups=mesh['fs'=16,'tp'=2] {'fs'}, dimensions={0} | all-to-all | bytes 1441792 | tf_op jit(solution)/shard_map/all_to_all | solution.py:21
  88.5 1.2 broadcast_in_dim.29
  89.8 0.4 copy-done.4
  90.1 0.4 copy.46
  90.6 1.8 copy.48
  92.4 1.6 fusion.4
  94.0 2.5 fusion.14
  96.5 0.6 all-gather.11.cloned.1.call-done
  97.1 5.5 %fusion.10 = f32[256,2048]{1,0:T(8,128)} fusion(bf16[352,2048]{1,0:T(8,128)(2,1)} %bitcast.68, bf16[352,2048]{1,0:T(8,128)(2,1)} %bitcast.67, bf16[1,256,2048]{2,1,0:T(8,128)(2,1)} %param.9, f32[256]{0:T(256)S(1)} %add_rsqrt_fusion.1, f32[256,352]{0,1:T(8,128)S(1)} %fusion.14), kind=kOutput, calls=%fused_computation.20 | convolution fusion | flops 740311040 | bytes 6390784 | tf_op jit(solution)/shard_map/dot_general | solution.py:68
  102.7 0.6 copy-done.13
  103.3 1.1 multiply_convert_fusion.1
  104.3 41.4 %all_to_all.99 = bf16[16,176,128]{2,1,0:T(8,128)(2,1)S(1)} all-to-all(bf16[16,176,128]{2,1,0:T(8,128)(2,1)S(1)} %bitcast.57), channel_id=1, replica_groups=mesh['fs'=16,'tp'=2] {'fs'}, dimensions={0} | all-to-all | bytes 1441792 | tf_op jit(solution)/shard_map/all_to_all | solution.py:19
  145.9 1.2 broadcast_in_dim.30
  147.2 26.7 %all_to_all.100 = bf16[16,176,128]{2,1,0:T(8,128)(2,1)S(1)} all-to-all(bf16[16,176,128]{2,1,0:T(8,128)(2,1)S(1)} %bitcast.55), channel_id=1, replica_groups=mesh['fs'=16,'tp'=2] {'fs'}, dimensions={0} | all-to-all | bytes 1441792 | tf_op jit(solution)/shard_map/all_to_all | solution.py:20
  174.1 1.2 broadcast_in_dim.31
  175.3 0.4 copy-done.5
  175.7 0.3 copy.50
  176.0 23.5 %all_to_all.101 = bf16[16,176,128]{2,1,0:T(8,128)(2,1)S(1)} all-to-all(bf16[16,176,128]{2,1,0:T(8,128)(2,1)S(1)} %bitcast.65), channel_id=1, replica_groups=mesh['fs'=16,'tp'=2] {'fs'}, dimensions={0} | all-to-all | bytes 1441792 | tf_op jit(solution)/shard_map/all_to_all | solution.py:21
  199.7 1.2 broadcast_in_dim.32
  201.2 50.3 %all-reduce.2.cloned.1.call-done = f32[256,2048]{1,0:T(8,128)} async-done(((f32[256,2048]{1,0:T(8,128)}), f32[256,2048]{1,0:T(8,128)}) %all-reduce.2.cloned.1.call-update) | async-done | bytes 2097168 | tf_op jit(solution)/shard_map/psum | solution.py:69
  251.4 2.1 fusion.2
  253.6 8.7 %all-gather.13.cloned.1.call-done = bf16[2,176,2048]{2,1,0:T(8,128)(2,1)} async-done(((bf16[1,176,2048]{2,1,0:T(8,128)(2,1)}), bf16[2,176,2048]{2,1,0:T(8,128)(2,1)}) %all-gather.13.cloned.1.call-update) | async-done | bytes 1441808 | tf_op jit(solution)/shard_map/all_gather | solution.py:24
  262.3 2.0 fusion.18
  264.3 10.8 %all-gather.15.cloned.1.call-done = bf16[2,176,2048]{2,1,0:T(8,128)(2,1)} async-done(((bf16[1,176,2048]{2,1,0:T(8,128)(2,1)}), bf16[2,176,2048]{2,1,0:T(8,128)(2,1)}) %all-gather.15.cloned.1.call-update) | async-done | bytes 1441808 | tf_op jit(solution)/shard_map/all_gather | solution.py:25
  275.1 12.9 %all-gather.17.cloned.1.call-done = bf16[2,176,2048]{2,1,0:T(8,128)(2,1)} async-done(((bf16[1,176,2048]{2,1,0:T(8,128)(2,1)}), bf16[2,176,2048]{2,1,0:T(8,128)(2,1)}) %all-gather.17.cloned.1.call-update) | async-done | bytes 1441808 | tf_op jit(solution)/shard_map/all_gather | solution.py:26
  288.0 5.2 %fusion.9 = f32[256,2048]{1,0:T(8,128)} fusion(bf16[352,2048]{1,0:T(8,128)(2,1)} %bitcast.71, bf16[352,2048]{1,0:T(8,128)(2,1)} %bitcast.70, bf16[256,2048]{1,0:T(8,128)(2,1)S(1)} %get-tuple-element.8, f32[256]{0:T(256)S(1)} %add_rsqrt_fusion, f32[256,352]{0,1:T(8,128)S(1)} %fusion.18), kind=kOutput, calls=%fused_computation.19 | convolution fusion | flops 740311040 | bytes 6390784 | tf_op jit(solution)/shard_map/dot_general | solution.py:39
  293.3 82.9 %reduce-scatter.2.cloned.1.call-done = f32[16,2048]{1,0:T(8,128)} async-done(((f32[256,2048]{1,0:T(8,128)}), f32[16,2048]{1,0:T(8,128)}) %reduce-scatter.2.cloned.1.call-update) | async-done | bytes 131088 | tf_op jit(solution)/shard_map/reduce_scatter | solution.py:74
  376.2 1.6 fusion.32
  377.7 1.1 copy.59
  378.8 0.8 copy-done.7
  379.6 1.1 copy.60
  380.7 0.8 copy-done.8
  381.5 1.1 copy.61
  382.6 0.8 copy-done.9
  383.4 1.1 copy.62
  384.5 0.8 copy-done.10
  385.3 1.1 copy.63
  386.4 0.8 copy-done.11
  387.1 1.1 copy.64
  (45 shorter events, 1.9 us)
Async XLA Ops:
  7.2 86.8 %all-gather.7.cloned.1.call-start = ((), (), s32[]{:S(2)}) async-start(), calls=%async_computation.7 | async-start | bytes 2162688 | tf_op jit(solution)/shard_map/all_gather | solution.py:24
  9.0 1.8 copy-start.12
  40.2 1.3 copy-start.1
  41.4 55.1 %all-gather.9.cloned.1.call-start = ((), (), s32[]{:S(2)}) async-start(), calls=%async_computation.8 | async-start | bytes 2162688 | tf_op jit(solution)/shard_map/all_gather | solution.py:25
  64.0 1.6 copy-start.3
  65.2 31.9 %all-gather.11.cloned.1.call-start = ((), (), s32[]{:S(2)}) async-start(), calls=%async_computation.9 | async-start | bytes 2162688 | tf_op jit(solution)/shard_map/all_gather | solution.py:26
  88.5 1.6 copy-start.4
  89.7 161.7 %all-reduce.2.cloned.1.call-start = ((), (), s32[]{:S(2)}) async-start(), calls=%async_computation.10 | async-start | bytes 4194304 | tf_op jit(solution)/shard_map/psum | solution.py:69
  102.6 0.7 copy-start.13
  102.6 159.6 %all-gather.13.cloned.1.call-start = ((), (), s32[]{:S(2)}) async-start(), calls=%async_computation.11 | async-start | bytes 2162688 | tf_op jit(solution)/shard_map/all_gather | solution.py:24
  145.9 1.3 copy-start.2
  147.1 127.9 %all-gather.15.cloned.1.call-start = ((), (), s32[]{:S(2)}) async-start(), calls=%async_computation.12 | async-start | bytes 2162688 | tf_op jit(solution)/shard_map/all_gather | solution.py:25
  174.1 1.6 copy-start.5
  175.3 112.7 %all-gather.17.cloned.1.call-start = ((), (), s32[]{:S(2)}) async-start(), calls=%async_computation.13 | async-start | bytes 2162688 | tf_op jit(solution)/shard_map/all_gather | solution.py:26
  199.7 51.7 %copy-start = (bf16[1,256,2048]{2,1,0:T(8,128)(2,1)S(1)}, bf16[1,256,2048]{2,1,0:T(8,128)(2,1)}, u32[]{:S(2)}) copy-start(bf16[1,256,2048]{2,1,0:T(8,128)(2,1)} %param.9) | copy-start | bytes 3145732
  200.9 175.2 %reduce-scatter.2.cloned.1.call-start = ((), (), s32[]{:S(2)}) async-start(), calls=%async_computation.14 | async-start | bytes 2228224 | tf_op jit(solution)/shard_map/reduce_scatter | solution.py:74
  293.2 84.5 %copy-start.6 = (bf16[2,176,2048]{2,1,0:T(8,128)(2,1)S(1)}, bf16[2,176,2048]{2,1,0:T(8,128)(2,1)}, u32[]{:S(2)}) copy-start(bf16[2,176,2048]{2,1,0:T(8,128)(2,1)} %all-gather.7.cloned.1.call-done) | copy-start | bytes 4325380
  377.7 1.9 copy-start.7
  379.6 1.9 copy-start.8
  381.5 1.9 copy-start.9
  383.4 1.9 copy-start.10
  385.3 1.9 copy-start.11
Sparse Core Ops, SparseCore 0:
  41.6 7.2 all-gather.6
  65.3 7.2 all-gather.8
  89.8 7.2 all-gather.10
  102.8 148.6 all-reduce.1
  253.4 8.8 all-gather.12
  264.3 10.7 all-gather.14
  277.2 10.7 all-gather.16
  293.4 82.7 reduce-scatter.1
where the time goes:
time: 396 us; the launch traced here: 395 us
  waiting for transfers between devices  166 us (42%)
  blocking collectives  164 us (41%)
  local copies, waits for them, and re-layouts  26.9 us (7%)
  matrix products  15.3 us (4%)
  between operations  14.3 us (4%)
  other arithmetic  7.42 us (2%)
    reduce_scatter x1, waiting for transfers between devices, shards(): lax.psum_scatter(projector(hidden_second, down_flat_two), 'fs', scatter_d...  82.9 us
    all_to_all x2, blocking collectives, relayout(): lax.all_to_all(gate_part, 'fs', split_axis=0, concat_axis=1, tiled=True)  69.5 us
    psum x1, waiting for transfers between devices, shards(): branch = lax.psum(partial_value, 'fs')  50.3 us
    all_to_all x2, blocking collectives, relayout(): lax.all_to_all(up_part, 'fs', split_axis=0, concat_axis=1, tiled=True)  49 us
    all_to_all x2, blocking collectives, relayout(): lax.all_to_all(down_part, 'fs', split_axis=0, concat_axis=1, tiled=True)  45.8 us
    unnamed x40, local copies, waits for them, and re-layouts  18.8 us
    all_gather x2, waiting for transfers between devices, relayout(): lax.all_gather(down_cut[None], 'tp', axis=0, tiled=True)  13.5 us
    all_gather x2, waiting for transfers between devices, relayout(): lax.all_gather(up_cut[None], 'tp', axis=0, tiled=True)  10.8 us
  transfers between devices with their start and end apart: 8, of which 6 were waited for; matrix products, arithmetic and copies ran while one was open for 5% of the time, Pallas kernels for 0%

commit v1 on v0

--- a/solution.py
+++ b/solution.py
@@ -1,6 +1,11 @@
+import functools
+import math
+
 import jax
 import jax.numpy as jnp
 from jax import lax
+from jax.experimental import pallas as pl
+from jax.experimental.pallas import tpu as pltpu
 from jax.sharding import PartitionSpec as P
 
 
@@ -78,29 +83,404 @@
     return (mixed, gate_one, up_one, down_one, gate_two, up_two, down_two)
 
 
+def loop(lo, hi, body):
+    lax.fori_loop(lo, hi, lambda i, c: (body(i), c)[1], 0)
+
+
+def step_kernel(
+    n,
+    inner,
+    tokens_ref,
+    gain_one_ref,
+    gain_two_ref,
+    w0,
+    w1,
+    w2,
+    w3,
+    w4,
+    w5,
+    mixed_ref,
+    o0,
+    o1,
+    o2,
+    o3,
+    o4,
+    o5,
+    raw,
+    cut,
+    served,
+    normed,
+    gate_acc,
+    up_acc,
+    hidden,
+    middle,
+    part,
+    plane_in,
+    plane_sum,
+    line_in,
+    load_sem,
+    store_sem,
+    send_sem,
+    recv_sem,
+    pass_send,
+    pass_recv,
+    ring_send,
+    ring_recv,
+):
+    outer = n // inner
+    me = lax.axis_index("fs")
+    core = lax.axis_index("tp")
+    row = me // inner
+    col = lax.rem(me, inner)
+    weights = (w0, w1, w2, w3, w4, w5)
+    outs = (o0, o1, o2, o3, o4, o5)
+    rows = served.shape[2]
+    feats = cut.shape[2]
+    depth = normed.shape[1]
+    mine = pl.ds(pl.multiple_of(me * feats, feats), feats)
+
+    def load(a):
+        return pltpu.make_async_copy(weights[a], raw.at[a], load_sem.at[a])
+
+    def store(a):
+        return pltpu.make_async_copy(served.at[a], outs[a], store_sem.at[a])
+
+    def cast(a):
+        load(a).wait()
+        gain = gain_one_ref if a < 3 else gain_two_ref
+
+        def tile(i):
+            at = pl.ds(pl.multiple_of(i * 128, 128), 128)
+            block = raw[a, :, at].T
+            if a % 3 != 2:
+                block = block * gain[...]
+            cut[a, at, :] = block.astype(jnp.bfloat16)
+
+        loop(0, raw.shape[2] // 128, tile)
+        served[a, core, :, mine] = cut[a, pl.ds(pl.multiple_of(me * rows, rows), rows), :]
+
+    def block_copy(a, j):
+        k = lax.rem(j, outer) * inner + j // outer
+        to = lax.rem(me + k, n)
+        return pltpu.make_async_remote_copy(
+            src_ref=cut.at[a, pl.ds(pl.multiple_of(to * rows, rows), rows), :],
+            dst_ref=served.at[a, core, :, mine],
+            send_sem=send_sem.at[a, j],
+            recv_sem=recv_sem.at[a, j],
+            device_id={"fs": to},
+            device_id_type=pl.DeviceIdType.MESH,
+        )
+
+    def send(a):
+        loop(1, n, lambda j: block_copy(a, j).start())
+
+    def pass_copy(a):
+        return pltpu.make_async_remote_copy(
+            src_ref=served.at[a, core],
+            dst_ref=served.at[a, core],
+            send_sem=pass_send.at[a],
+            recv_sem=pass_recv.at[a],
+            device_id={"tp": 1 - core},
+            device_id_type=pl.DeviceIdType.MESH,
+        )
+
+    def arrive(a):
+        loop(1, n, lambda j: block_copy(a, j).wait_recv())
+        pass_copy(a).start()
+
+    def complete(a):
+        pass_copy(a).wait_recv()
+        store(a).start()
+
+    def ring_copy(stage, k, src, dst, to):
+        return pltpu.make_async_remote_copy(
+            src_ref=src,
+            dst_ref=dst,
+            send_sem=ring_send.at[stage, k],
+            recv_sem=ring_recv.at[stage, k],
+            device_id={"fs": to},
+            device_id_type=pl.DeviceIdType.MESH,
+        )
+
+    def plane_copies(half):
+        copies = []
+        for k in range(1, inner):
+            to = lax.rem(col + k, inner)
+            copies.append(
+                ring_copy(half, k, part.at[half, to], plane_in.at[half, k - 1], row * inner + to)
+            )
+        return copies
+
+    def line_copies(half):
+        copies = []
+        for k in range(1, outer):
+            to = lax.rem(row + k, outer)
+            copies.append(
+                ring_copy(
+                    2 + half, k, plane_sum.at[half, to], line_in.at[half, k - 1], to * inner + col
+                )
+            )
+        return copies
+
+    def spread_line():
+        spot = middle.at[col, row]
+        return [
+            ring_copy(4, k, spot, spot, lax.rem(row + k, outer) * inner + col)
+            for k in range(1, outer)
+        ]
+
+    def spread_plane():
+        spot = middle.at[col]
+        return [
+            ring_copy(5, k, spot, spot, row * inner + lax.rem(col + k, inner))
+            for k in range(1, inner)
+        ]
+
+    keep = tokens_ref.shape[2]
+
+    def normalize_rows(source):
+        def one(i):
+            wide = source[i // outer, lax.rem(i, outer)].astype(jnp.float32)
+            scale = lax.rsqrt(jnp.mean(wide * wide, axis=-1, keepdims=True) + 1e-06)
+            at = pl.ds(pl.multiple_of(i * keep, keep), keep)
+            normed[at, :] = (wide * scale).astype(jnp.bfloat16)
+
+        loop(0, n, one)
+
+    def expand(g, u):
+        gate_acc[...] = jnp.zeros_like(gate_acc)
+        up_acc[...] = jnp.zeros_like(up_acc)
+        wide = 256
+
+        def one(i):
+            at = pl.ds(pl.multiple_of(i * wide, wide), wide)
+            left = normed[:, at]
+            for acc, a in ((gate_acc, g), (up_acc, u)):
+                right = served[a, :, :, at].reshape(-1, wide)
+                acc[...] += lax.dot_general(
+                    left, right, (((1,), (1,)), ((), ())), preferred_element_type=jnp.float32
+                )
+
+        loop(0, depth // wide, one)
+        gate = gate_acc[...]
+        hidden[...] = (gate / (1.0 + jnp.exp(-gate)) * up_acc[...]).astype(jnp.bfloat16)
+
+    def contract(d, half):
+        wide = 256
+
+        def one(i):
+            at = pl.ds(pl.multiple_of(i * wide, wide), wide)
+            right = served[d, :, :, at].reshape(-1, wide)
+            value = jnp.dot(hidden[...], right, preferred_element_type=jnp.float32)
+            part[half, :, :, :, at] = value.astype(jnp.bfloat16).reshape(inner, outer, keep, wide)
+
+        loop(0, depth // wide, one)
+
+    def sum_plane(half):
+        def one(i):
+            total = part[half, col, i].astype(jnp.float32)
+            for k in range(inner - 1):
+                total += plane_in[half, k, i].astype(jnp.float32)
+            plane_sum[half, i] = total.astype(jnp.bfloat16)
+
+        loop(0, outer, one)
+
+    def sum_line(half):
+        total = plane_sum[half, row].astype(jnp.float32)
+        for k in range(outer - 1):
+            total += line_in[half, k].astype(jnp.float32)
+        return total
+
+    def start(copies):
+        for copy in copies:
+            copy.start()
+
+    def receive(copies):
+        for copy in copies:
+            copy.wait_recv()
+
+    for a in range(6):
+        load(a).start()
+    for a in range(4):
+        cast(a)
+        send(a)
+    cast(4)
+    cast(5)
+    normalize_rows(tokens_ref)
+    arrive(0)
+    arrive(1)
+    complete(0)
+    complete(1)
+    expand(0, 1)
+    arrive(2)
+    complete(2)
+    contract(2, 0)
+    start(plane_copies(0))
+    send(4)
+    receive(plane_copies(0))
+    sum_plane(0)
+    start(line_copies(0))
+    receive(line_copies(0))
+    own = tokens_ref[col, row].astype(jnp.float32) + 0.5 * sum_line(0)
+    middle[col, row] = own.astype(jnp.bfloat16)
+    start(spread_line())
+    receive(spread_line())
+    start(spread_plane())
+    send(5)
+    arrive(3)
+    receive(spread_plane())
+    normalize_rows(middle)
+    arrive(4)
+    complete(3)
+    complete(4)
+    expand(3, 4)
+    arrive(5)
+    complete(5)
+    contract(5, 1)
+    start(plane_copies(1))
+    receive(plane_copies(1))
+    sum_plane(1)
+    start(line_copies(1))
+    receive(line_copies(1))
+    last = middle[col, row].astype(jnp.float32) + 0.5 * sum_line(1)
+    mixed_ref[...] = last.astype(jnp.bfloat16)
+
+    for a in range(6):
+        store(a).wait()
+        pass_copy(a).wait_send()
+        loop(1, n, lambda j, a=a: block_copy(a, j).wait_send())
+    for copies in (
+        plane_copies(0),
+        plane_copies(1),
+        line_copies(0),
+        line_copies(1),
+        spread_line(),
+        spread_plane(),
+    ):
+        for copy in copies:
+            copy.wait_send()
+
+
+def hand_on(*refs):
+    half = len(refs) // 2
+    for source, target in zip(refs[:half], refs[half:]):
+        target[...] = source[...]
+
+
+def fused_shards(tokens, gain_first, gate_first, up_first, down_first,
+                 gain_second, gate_second, up_second, down_second):
+    n = lax.axis_size("fs")
+    tp = lax.axis_size("tp")
+    inner = math.isqrt(n)
+    outer = n // inner
+    feats, units = gate_first.shape
+    rows = units // n
+    plen, depth = tokens.shape[1], tokens.shape[2]
+    keep = plen // n
+    bf16, f32 = jnp.bfloat16, jnp.float32
+    shuffled = tokens[0].reshape(outer, inner, keep, depth).transpose(1, 0, 2, 3)
+    vmem = pl.BlockSpec(memory_space=pltpu.VMEM)
+    anywhere = pl.BlockSpec(memory_space=pl.ANY)
+    served_shape = jax.ShapeDtypeStruct((tp, rows, depth), bf16)
+    hid = tp * rows
+    dma = pltpu.SemaphoreType.DMA
+    width = max(inner, outer)
+    results = pl.pallas_call(
+        functools.partial(step_kernel, n, inner),
+        out_shape=(jax.ShapeDtypeStruct((keep, depth), bf16),) + (served_shape,) * 6,
+        in_specs=[vmem] * 3 + [anywhere] * 6,
+        out_specs=(vmem,) + (anywhere,) * 6,
+        scratch_shapes=[
+            pltpu.VMEM((6, feats, units), f32),
+            pltpu.VMEM((6, units, feats), bf16),
+            pltpu.VMEM((6, tp, rows, depth), bf16),
+            pltpu.VMEM((plen, depth), bf16),
+            pltpu.VMEM((plen, hid), f32),
+            pltpu.VMEM((plen, hid), f32),
+            pltpu.VMEM((plen, hid), bf16),
+            pltpu.VMEM((inner, outer, keep, depth), bf16),
+            pltpu.VMEM((2, inner, outer, keep, depth), bf16),
+            pltpu.VMEM((2, inner - 1, outer, keep, depth), bf16),
+            pltpu.VMEM((2, outer, keep, depth), bf16),
+            pltpu.VMEM((2, outer - 1, keep, depth), bf16),
+            dma((6,)),
+            dma((6,)),
+            dma((6, n)),
+            dma((6, n)),
+            dma((6,)),
+            dma((6,)),
+            dma((6, width)),
+            dma((6, width)),
+        ],
+        compiler_params=pltpu.CompilerParams(
+            has_side_effects=True, vmem_limit_bytes=58 * 1024 * 1024
+        ),
+    )(
+        shuffled,
+        gain_first.reshape(1, feats),
+        gain_second.reshape(1, feats),
+        gate_first,
+        up_first,
+        down_first,
+        gate_second,
+        up_second,
+        down_second,
+    )
+    block = pl.BlockSpec((1, rows, depth // 2), lambda i, j: (i, 0, j))
+    copies = pl.pallas_call(
+        hand_on,
+        grid=(tp, 2),
+        out_shape=(served_shape,) * 6,
+        in_specs=[block] * 6,
+        out_specs=(block,) * 6,
+    )(*results[1:])
+    return (results[0][None],) + tuple(copies)
+
+
+def fits(mesh, tokens, gate):
+    n, tp = mesh.shape["fs"], mesh.shape["tp"]
+    inner = math.isqrt(n)
+    depth, hidden = gate.shape
+    plen = tokens.shape[1]
+    if tp != 2 or inner < 2 or n % inner or depth % (n * 128) or hidden % (tp * n * 16):
+        return False
+    if depth % 256 or (hidden // tp) % 128 or plen % (n * 16) or tokens.shape[0] != tp:
+        return False
+    local = depth // n * (hidden // tp)
+    need = local * 6 * 4 + local * 6 * 2 + local * 6 * 2 * tp
+    need += plen * depth * 2 * 10 + plen * (hidden // n) * 12
+    return need < 40 * 1024 * 1024
+
+
 def solution(mesh):
-    return jax.shard_map(
-        shards,
-        mesh=mesh,
-        in_specs=(
-            P("tp", None, None),
-            P("fs"),
-            P("fs", "tp"),
-            P("fs", "tp"),
-            P("fs", "tp"),
-            P("fs"),
-            P("fs", "tp"),
-            P("fs", "tp"),
-            P("fs", "tp"),
-        ),
-        out_specs=(
-            P("tp", "fs", None),
-            P(None, "fs", None),
-            P(None, "fs", None),
-            P(None, "fs", None),
-            P(None, "fs", None),
-            P(None, "fs", None),
-            P(None, "fs", None),
-        ),
-        check_vma=False,
-    )
+    def run(body):
+        return jax.shard_map(
+            body,
+            mesh=mesh,
+            in_specs=(
+                P("tp", None, None),
+                P("fs"),
+                P("fs", "tp"),
+                P("fs", "tp"),
+                P("fs", "tp"),
+                P("fs"),
+                P("fs", "tp"),
+                P("fs", "tp"),
+                P("fs", "tp"),
+            ),
+            out_specs=(
+                P("tp", "fs", None),
+                P(None, "fs", None),
+                P(None, "fs", None),
+                P(None, "fs", None),
+                P(None, "fs", None),
+                P(None, "fs", None),
+                P(None, "fs", None),
+            ),
+            check_vma=False,
+        )
+
+    def step(*args):
+        return run(fused_shards if fits(mesh, args[0], args[2]) else shards)(*args)
+
+    return step

time: 396 us -> 174 us (0.44)
  Pallas kernels: 0 us -> 170 us
  waiting for transfers between devices: 166 us -> 0 us
  blocking collectives: 164 us -> 0 us
  local copies, waits for them, and re-layouts: 26.9 us -> 2.94 us
  matrix products: 15.3 us -> 0 us
  between operations: 14.3 us -> 0.66 us
  other arithmetic: 7.42 us -> 0 us
    pallas_call x0 -> x2, Pallas kernels: none -> 170 us  [the longest x1 163 us: fused_shards(): pl.pallas_call(functools.partial(step_kernel, n, inner), out_shape=(jax.S...]
    all_to_all x6 -> x0, blocking collectives: 164 us -> none  [the longest x2 69.5 us: relayout(): lax.all_to_all(gate_part, 'fs', split_axis=0, concat_axis=1, tiled=True)]
    reduce_scatter x1 -> x0, waiting for transfers between devices: 82.9 us -> none  [shards(): lax.psum_scatter(projector(hidden_second, down_flat_two), 'fs', scatter_d...]
    psum x1 -> x0, waiting for transfers between devices: 50.3 us -> none  [shards(): branch = lax.psum(partial_value, 'fs')]
    all_gather x6 -> x0, waiting for transfers between devices: 33 us -> none  [the longest x2 13.5 us: relayout(): lax.all_gather(down_cut[None], 'tp', axis=0, tiled=True)]
    unnamed x40 -> x3, local copies, waits for them, and re-layouts: 18.8 us -> 0.64 us
    dot_general x4 -> x0, matrix products: 15.3 us -> none  [the longest x1 5.52 us: shards(): jnp.dot(hidden_first, down_flat_one, preferred_element_type=jnp.float32)]
    broadcast_in_dim x6 -> x0, local copies, waits for them, and re-layouts: 6.98 us -> none  [the longest x2 2.33 us: relayout(): up_cut[None]]
  transfers between devices with their start and end apart: 8 -> 0, of which waited for: 6 -> 0; matrix products, arithmetic and copies ran while one was open for 5% -> 0% of each run, Pallas kernels for 0% -> 0%
where the time goes in v1:
time: 174 us
  Pallas kernels  170 us (98%)
  local copies, waits for them, and re-layouts  2.94 us (2%)
    pallas_call x1, Pallas kernels, fused_shards(): pl.pallas_call(functools.partial(step_kernel, n, inner), out_shape=(jax.S...  163 us
    pallas_call x1, Pallas kernels, fused_shards(): pl.pallas_call(hand_on, grid=(tp, 2), out_shape=(served_shape,) * 6, in_s...  7.1 us

profile of v1, /device:TPU:0, one launch (start us, length us, event | category | flops | bytes accessed | tf_op | source)
XLA Modules:
  0.0 173.5 jit_solution(8260928172318022203)
XLA Ops:
  0.6 2.3 %copy.18 = bf16[4,4,16,2048]{3,2,0,1:T(8,128)(2,1)} copy(bf16[4,4,16,2048]{3,2,1,0:T(8,128)(2,1)} %bitcast.8) | data formatting | bytes 2097152 | tf_op jit(solution)/shard_map/reshape;squeeze | solution.py:381
  2.9 162.8 %shard_map.144 = (bf16[16,2048]{1,0:T(8,128)(2,1)}, bf16[2,176,2048]{2,1,0:T(8,128)(2,1)}, bf16[2,176,2048]{2,1,0:T(8,128)(2,1)}, bf16[2,176,2048]{2,1,0:T(8,128...) custom-call(bf16[4,4,16,2048]{3,2,1,0:T(8,128)(2,1)} %bitcast.7, ...), custom_call_target="tpu_custom_call" | custom-call | tf_op jit(solution)/shard_map/pallas_call | solution.py:388
  165.8 0.0 copy-start
  165.8 7.1 %shard_map.145 = (bf16[2,176,2048]{2,1,0:T(8,128)(2,1)}, bf16[2,176,2048]{2,1,0:T(8,128)(2,1)}, bf16[2,176,2048]{2,1,0:T(8,128)(2,1)}, bf16[2,176,2048]{2,1,0:T(...) custom-call(bf16[2,176,2048]{2,1,0:T(8,128)(2,1)} %get-tuple-element.21.refs_0_, ...), custom_call_target="tpu_custom_call" | custom-call | tf_op jit(solution)/shard_map/pallas_call | solution.py:430
  172.9 0.0 copy-done
  172.9 0.6 copy.20
Async XLA Ops:
  165.8 7.1 %copy-start = (bf16[16,2048]{1,0:T(8,128)(2,1)S(1)}, bf16[16,2048]{1,0:T(8,128)(2,1)}, u32[]{:S(2)}) copy-start(bf16[16,2048]{1,0:T(8,128)(2,1)} %get-tuple-element.20) | copy-start | bytes 196612

commit v2 on v1

--- a/solution.py
+++ b/solution.py
@@ -149,14 +149,19 @@
         load(a).wait()
         gain = gain_one_ref if a < 3 else gain_two_ref
 
+        count = raw.shape[2] // 128
+        per = next(d for d in (11, 4, 2, 1) if count % d == 0)
+        spread = jnp.broadcast_to(gain[...], (128, feats)).T
+
         def tile(i):
-            at = pl.ds(pl.multiple_of(i * 128, 128), 128)
-            block = raw[a, :, at].T
-            if a % 3 != 2:
-                block = block * gain[...]
-            cut[a, at, :] = block.astype(jnp.bfloat16)
-
-        loop(0, raw.shape[2] // 128, tile)
+            for piece in range(per):
+                at = pl.ds(pl.multiple_of((i * per + piece) * 128, 128), 128)
+                block = raw[a, :, at]
+                if a % 3 != 2:
+                    block = block * spread
+                cut[a, at, :] = block.astype(jnp.bfloat16).T
+
+        loop(0, count // per, tile)
         served[a, core, :, mine] = cut[a, pl.ds(pl.multiple_of(me * rows, rows), rows), :]
 
     def block_copy(a, j):
@@ -238,9 +243,9 @@
 
     keep = tokens_ref.shape[2]
 
-    def normalize_rows(source):
+    def normalize_rows(pick):
         def one(i):
-            wide = source[i // outer, lax.rem(i, outer)].astype(jnp.float32)
+            wide = pick(i // outer, lax.rem(i, outer)).astype(jnp.float32)
             scale = lax.rsqrt(jnp.mean(wide * wide, axis=-1, keepdims=True) + 1e-06)
             at = pl.ds(pl.multiple_of(i * keep, keep), keep)
             normed[at, :] = (wide * scale).astype(jnp.bfloat16)
@@ -306,7 +311,7 @@
         send(a)
     cast(4)
     cast(5)
-    normalize_rows(tokens_ref)
+    normalize_rows(lambda c, r: tokens_ref[r, c])
     arrive(0)
     arrive(1)
     complete(0)
@@ -321,7 +326,7 @@
     sum_plane(0)
     start(line_copies(0))
     receive(line_copies(0))
-    own = tokens_ref[col, row].astype(jnp.float32) + 0.5 * sum_line(0)
+    own = tokens_ref[row, col].astype(jnp.float32) + 0.5 * sum_line(0)
     middle[col, row] = own.astype(jnp.bfloat16)
     start(spread_line())
     receive(spread_line())
@@ -329,7 +334,7 @@
     send(5)
     arrive(3)
     receive(spread_plane())
-    normalize_rows(middle)
+    normalize_rows(lambda c, r: middle[c, r])
     arrive(4)
     complete(3)
     complete(4)
@@ -378,7 +383,7 @@
     plen, depth = tokens.shape[1], tokens.shape[2]
     keep = plen // n
     bf16, f32 = jnp.bfloat16, jnp.float32
-    shuffled = tokens[0].reshape(outer, inner, keep, depth).transpose(1, 0, 2, 3)
+    shuffled = tokens[0].reshape(outer, inner, keep, depth)
     vmem = pl.BlockSpec(memory_space=pltpu.VMEM)
     anywhere = pl.BlockSpec(memory_space=pl.ANY)
     served_shape = jax.ShapeDtypeStruct((tp, rows, depth), bf16)

time: 174 us -> 169 us (0.971)
  local copies, waits for them, and re-layouts: 2.94 us -> 0.64 us
  Pallas kernels: 170 us -> 168 us
    another operation x1 -> x0, local copies, waits for them, and re-layouts: 2.3 us -> none  [fused_shards(): tokens[0].reshape(outer, inner, keep, depth).transpose(1, 0, 2, 3)]
    pallas_call x1, Pallas kernels: 163 us -> 161 us  [fused_shards(): pl.pallas_call(functools.partial(step_kernel, n, inner), out_shape=(jax.S...]
where the time goes in v2:
time: 169 us
  Pallas kernels  168 us (99%)
    pallas_call x1, Pallas kernels, fused_shards(): pl.pallas_call(functools.partial(step_kernel, n, inner), out_shape=(jax.S...  161 us
    pallas_call x1, Pallas kernels, fused_shards(): pl.pallas_call(hand_on, grid=(tp, 2), out_shape=(served_shape,) * 6, in_s...  7.1 us

profile of v2, /device:TPU:0, one launch (start us, length us, event | category | flops | bytes accessed | tf_op | source)
XLA Modules:
  0.0 169.3 jit_solution(1170256936210309153)
XLA Ops:
  0.6 160.9 %shard_map.144 = (bf16[16,2048]{1,0:T(8,128)(2,1)}, bf16[2,176,2048]{2,1,0:T(8,128)(2,1)}, bf16[2,176,2048]{2,1,0:T(8,128)(2,1)}, bf16[2,176,2048]{2,1,0:T(8,128...) custom-call(bf16[4,4,16,2048]{3,2,1,0:T(8,128)(2,1)} %bitcast.4, ...), custom_call_target="tpu_custom_call" | custom-call | tf_op jit(solution)/shard_map/pallas_call | solution.py:393
  161.5 0.0 copy-start
  161.5 7.1 %shard_map.145 = (bf16[2,176,2048]{2,1,0:T(8,128)(2,1)}, bf16[2,176,2048]{2,1,0:T(8,128)(2,1)}, bf16[2,176,2048]{2,1,0:T(8,128)(2,1)}, bf16[2,176,2048]{2,1,0:T(...) custom-call(bf16[2,176,2048]{2,1,0:T(8,128)(2,1)} %get-tuple-element.21.refs_0_, ...), custom_call_target="tpu_custom_call" | custom-call | tf_op jit(solution)/shard_map/pallas_call | solution.py:435
  168.6 0.0 copy-done
  168.7 0.6 copy.17
Async XLA Ops:
  161.5 7.1 %copy-start = (bf16[16,2048]{1,0:T(8,128)(2,1)S(1)}, bf16[16,2048]{1,0:T(8,128)(2,1)}, u32[]{:S(2)}) copy-start(bf16[16,2048]{1,0:T(8,128)(2,1)} %get-tuple-element.20) | copy-start | bytes 196612
